TPU v7x, 512 devices: a whole 4x8x8 slice. The times are simulated.
512 devices in a mesh: sp: 64 (over z, y), dp: 8 (over x, core).
Axes of the slice: x: 4, y: 8, z: 8, core: 2. Of those that a mesh axis runs over, the one named last changes fastest.
Arguments:
- inputs: bfloat16 [8, 8192, 2048], P('dp', 'sp'), may hold values from -6 to 6
- conv_weight: bfloat16 [4, 2048], replicated, may hold values from -3 to 3
- gate_weight: bfloat16 [2, 8, 256, 256], P(None, 'dp'), may hold values from -0.375 to 0.375
- rate_param: float32 [2048], replicated, may hold values from 4 to 12.5
- pace: float32 [8, 8192], P('dp'), may hold values from 0.5 to 30000
Outputs:
- recurrent: bfloat16 [8, 8192, 2048], P('dp', 'sp')
All inputs are finite; a program needn't handle non-finite values.
Results may differ from a plain program's by a relative error of at most 0.008.
Values may be sent and summed in bfloat16 or wider, within the bound.
No kernel may reach another device: no remote copies, remote signals or barrier semaphores. Data moves between devices by JAX's collectives and lax.ppermute only.
A program may use at most 128 MiB of HBM per device.

v0:
```python
import jax
import jax.numpy as jnp
from jax import lax
from jax.sharding import Mesh
from jax.sharding import PartitionSpec as P

HEADS = 8
BLOCK = 256
CONV = 4
DP = ("dp_0", "dp_1")
gate_power = 8.0


def passed_along(array, axis, by):
    devices = lax.axis_size(axis)
    pairs = [(i, i + by) for i in range(devices) if 0 <= i + by < devices]
    return lax.ppermute(array, axis, pairs)


def piece_ends(length, count):
    unit = 8 if length >= 8 * count else 1
    return [length // unit * k // count * unit for k in range(1, count)]


def gather_in_order(array, axes, sequence):
    pieces = array[None]
    for k in sequence:
        pieces = lax.all_gather(pieces, axes[k], axis=0, tiled=True)
    block = [lax.axis_size(axes[k]) for k in reversed(sequence)]
    pieces = pieces.reshape(*block, *array.shape)
    turned = sorted(range(len(sequence)), key=lambda place: sequence[len(sequence) - 1 - place])
    return pieces.transpose(*turned, *range(len(sequence), pieces.ndim)).reshape(-1, *array.shape)


def joined_along(pieces, dim):
    lengths = list(pieces.shape[1:])
    lengths[dim] *= pieces.shape[0]
    return jnp.moveaxis(pieces, 0, dim).reshape(lengths)


def gather_all_axes(array, axes, dim):
    widest = max(range(max(1, array.ndim - 1)), key=lambda d: array.shape[d])
    count, outs = (len(axes), [])
    for leading, section in enumerate(
        jnp.split(array, piece_ends(array.shape[widest], count), axis=widest)
    ):
        if section.size:
            sequence = [(leading - k) % count for k in range(count)]
            outs.append(gather_in_order(section, axes, sequence))
    return joined_along(jnp.concatenate(outs, axis=widest + 1), dim)


def from_everyone(array, axis):
    copies = jnp.broadcast_to(array, (lax.axis_size(axis), *array.shape))
    return lax.all_to_all(copies, axis, split_axis=0, concat_axis=0, tiled=True)


def gathered_once(array, axis):
    leaves = jax.tree.leaves(array)
    sequence = sorted(range(len(leaves)), key=lambda k: -leaves[k].size)
    width = (1, *leaves[sequence[0]].shape)[-1]
    lines = [
        jnp.pad(leaves[k].reshape(-1), (0, -leaves[k].size % width)).reshape(-1, width)
        for k in sequence
    ]
    both, at, found = (from_everyone(jnp.concatenate(lines), axis), 0, {})
    for k, line in zip(sequence, lines):
        section = both[:, at : at + len(line)].reshape(len(both), -1)
        found[k] = section[:, : leaves[k].size].reshape(-1, *leaves[k].shape)
        at += len(line)
    numbers = iter(range(len(leaves)))
    return jax.tree.map(lambda _: found[next(numbers)], array)


def combined_pairwise(pieces, combine):
    while len(jax.tree.leaves(pieces)[0]) > 1:
        pieces = jax.vmap(combine)(
            *(jax.tree.map(lambda part: part[side::2], pieces) for side in (0, 1))
        )
    return jax.tree.map(lambda part: part[0], pieces)


def prefix(array, axis, combine, identity):
    devices, here = (lax.axis_size(axis), lax.axis_index(axis))
    passed = jnp.arange(devices) < here

    def kept(part, zero, own):
        part = jnp.where(
            passed.reshape(-1, *(1 for _ in own.shape)), part, jnp.asarray(zero, own.dtype)
        )
        return part

    pieces = gathered_once(array, axis)
    return combined_pairwise(jax.tree.map(kept, pieces, identity, array), combine)


def combine(earlier, later):
    decay_e, state_e = earlier
    decay_l, state_l = later
    return (decay_e * decay_l, decay_l * state_e + state_l)


def lru_terms(pre_recur, pre_input, values, rate_col, pace_col):
    recur_gate = jax.nn.sigmoid(pre_recur.astype(jnp.float32))
    input_gate = jax.nn.sigmoid(pre_input.astype(jnp.float32))
    log_decay = -gate_power * pace_col * recur_gate * jax.nn.softplus(-rate_col)
    decay = jnp.exp(log_decay)
    drive = jnp.sqrt(-jnp.expm1(2.0 * log_decay)) * input_gate * values.astype(jnp.float32)
    return (decay, drive)


def body(inputs, conv_weight, gate_weight, rate_param, pace):
    own_rows = inputs[0].T
    width = own_rows.shape[0]
    count = own_rows.shape[1]
    earlier = passed_along(own_rows[:, count - (CONV - 1) :], "sp", 1)
    padded = jnp.concatenate([earlier, own_rows], axis=1).astype(jnp.float32)
    conv_taps = conv_weight.astype(jnp.float32)
    conv_out = jnp.zeros((width, count), jnp.float32)
    for tap in range(CONV):
        conv_out = conv_out + conv_taps[tap][:, None] * padded[:, tap : tap + count]
    conv_out = conv_out.astype(jnp.bfloat16)
    by_head = conv_out.reshape(HEADS, BLOCK, count)
    preact = (
        jnp.einsum(
            "hit,ghij->ghjt",
            by_head,
            gather_all_axes(gate_weight, DP, 1),
            preferred_element_type=jnp.float32,
        )
        .astype(jnp.bfloat16)
        .reshape(2, width, count)
    )
    own_pace = lax.dynamic_slice_in_dim(pace[0], lax.axis_index("sp") * count, count)
    decay, drive = lru_terms(preact[0], preact[1], conv_out, rate_param[:, None], own_pace[None, :])
    decay_run, state = lax.associative_scan(combine, (decay, drive), axis=1)
    identity = (jnp.ones((width,), jnp.float32), jnp.zeros((width,), jnp.float32))
    _, carried = prefix((decay_run[:, -1], state[:, -1]), "sp", combine, identity)
    result = (state + decay_run * carried[:, None]).astype(jnp.bfloat16)
    return result.T[None]


def solution(mesh):
    finer = Mesh(mesh.devices.reshape(mesh.shape["sp"], 4, 2), ("sp", "dp_0", "dp_1"))
    in_specs = (P(DP, "sp", None), P(), P(None, DP, None, None), P(), P(DP, None))
    out_specs = P(DP, "sp", None)
    return jax.shard_map(body, mesh=finer, in_specs=in_specs, out_specs=out_specs, check_vma=False)
```

profile of v0, /device:TPU:8, one launch (start us, length us, event | category | flops | bytes accessed | tf_op | source)
XLA Modules:
  0.0 180.7 jit_solution(7112969151282541759)
XLA Ops:
  7.6 13.9 %all-gather = bf16[8,1,128,256]{3,2,1,0:T(8,128)(2,1)} all-gather(bf16[2,1,128,256]{3,2,1,0:T(8,128)(2,1)S(1)} %get-tuple-element.21), channel_id=2, replica_groups=mesh['sp'=64,'dp_0'=4,'dp_1'=2] {'dp_0'}, dimensions={0}, use_global_device_ids=true | all-gather | bytes 655360 | tf_op jit(solution)/shard_map/all_gather | solution.py:28
  21.5 2.1 %all-gather.1 = bf16[4,1,128,256]{3,2,1,0:T(8,128)(2,1)} all-gather(bf16[2,1,128,256]{3,2,1,0:T(8,128)(2,1)S(1)} %get-tuple-element.22), channel_id=3, replica_groups=mesh['sp'=64,'dp_0'=4,'dp_1'=2] {'dp_1'}, dimensions={0}, use_global_device_ids=true | all-gather | bytes 393216 | tf_op jit(solution)/shard_map/all_gather | solution.py:28
  23.7 3.5 %collective-permute-start = (bf16[2048,3]{0,1:T(4,128)(2,1)S(1)}, bf16[2048,3]{0,1:T(4,128)(2,1)S(1)}, u32[]{:S(2)}, u32[]{:S(2)}) collective-permute-start(bf16[2048,3]{0,1:T(4,128)(2,1)S(1)} %slice.422), channel_id=1, source_target_pairs={{0,8},{8,16},{16,24},{24,32},{32,40},{40,48},{48,56},{56,64},{64,7... | collective-permute-start | bytes 36872 | tf_op jit(solution)/shard_map/ppermute | solution.py:17
  28.0 4.3 %collective-permute-done = bf16[2048,3]{0,1:T(4,128)(2,1)S(1)} collective-permute-done((bf16[2048,3]{0,1:T(4,128)(2,1)S(1)}, bf16[2048,3]{0,1:T(4,128)(2,1)S(1)}, u32[]{:S(2)}, u32[]{:S(2)}) %collective-permute-start) | collective-permute-done | bytes 12320 | tf_op jit(solution)/shard_map/ppermute | solution.py:17
  33.9 9.5 %all-gather.5.cloned.1.call-done = bf16[8,2,1,128,256]{4,3,2,1,0:T(8,128)(2,1)} async-done(((bf16[4,2,1,128,256]{4,3,2,1,0:T(8,128)(2,1)}), bf16[8,2,1,128,256]{4,3,2,1,0:T(8,128)(2,1)}) %all-gather.5.cloned.1.call-update) | async-done | bytes 1048592 | tf_op jit(solution)/shard_map/all_gather | solution.py:28
  43.4 1.6 copy.16
  45.1 31.2 %all-gather.7.cloned.1.call-done = bf16[8,2,1,128,256]{4,3,2,1,0:T(8,128)(2,1)} async-done(((bf16[2,2,1,128,256]{4,3,2,1,0:T(8,128)(2,1)}), bf16[8,2,1,128,256]{4,3,2,1,0:T(8,128)(2,1)}) %all-gather.7.cloned.1.call-update) | async-done | bytes 1048592 | tf_op jit(solution)/shard_map/all_gather | solution.py:28
  76.3 1.6 copy.18
  77.9 1.7 fusion.4
  80.2 1.3 copy.21
  82.9 2.8 %convert_multiply_fusion = (f32[2048,128]{0,1:T(8,128)S(1)}, f32[2048,128]{0,1:T(8,128)S(1)}) fusion(f32[2048,128]{0,1:T(8,128)} %copy.21, f32[2048,128]{0,1:T(8,128)} %copy.20, f32[2048]{0:T(1024)S(1)} %compare_select_fusion, f32[128]{0:T(128)S(1)} %multiply_bitcast_fusion, f32[2048,131]{0,1:T(8,128)S(1)} %maximum_convert_fusion, f32[2048]{0:T(1024)S(1)} %bitcast.69, ...), kind=kLoop, calls=%fused_computation.15 | loop fusion | flops 3932160 | bytes 8430080 | tf_op jit(solution)/shard_map/mul | solution.py:108
  85.7 1.5 slice.380
  87.2 1.5 slice.334
  88.7 1.5 slice.333
  90.2 1.5 slice.336
  91.6 1.5 slice.332
  93.1 1.5 slice.331
  94.6 1.3 multiply_add_fusion
  102.7 2.1 %pad.99 = f32[2048,128]{0,1:T(8,128)S(1)} pad(f32[2048,64]{0,1:T(8,128)} %add.213, f32[]{:T(128)} %constant.8.clone.1), padding=0_0_0x1_0_1 | pad | bytes 1572868 | tf_op jit(solution)/shard_map/pad | solution.py:136
  104.8 4.6 %pad.113 = f32[2048,128]{0,1:T(8,128)} pad(f32[2048,64]{0,1:T(8,128)} %add.221, f32[]{:T(128)} %constant.8.clone.1), padding=0_0_0x1_0_1 | pad | bytes 1572868 | tf_op jit(solution)/shard_map/pad | solution.py:136
  110.4 1.5 broadcast_in_dim.37
  111.9 13.6 %all-to-all-start = ((f32[64,2,2048]{2,1,0:T(2,128)}), f32[64,2,2048]{2,1,0:T(2,128)}, u32[]{:S(2)}, u32[]{:S(2)}) async-start(f32[64,2,2048]{2,1,0:T(2,128)} %broadcast_in_dim.37), calls=%async_computation | async-start | bytes 2097152 | tf_op jit(solution)/shard_map/all_to_all | solution.py:55
  125.5 27.8 %all-to-all-done = f32[64,2,2048]{2,1,0:T(2,128)} async-done(((f32[64,2,2048]{2,1,0:T(2,128)}), f32[64,2,2048]{2,1,0:T(2,128)}, u32[]{:S(2)}, u32[]{:S(2)}) %all-to-all-start) | async-done | bytes 1048608 | tf_op jit(solution)/shard_map/all_to_all | solution.py:55
  153.2 2.6 %fusion.22 = (f32[64,1,2048]{2,1,0:T(1,128)S(1)}, f32[64,1,2048]{2,1,0:T(1,128)S(1)}) fusion(f32[64,2,2048]{2,1,0:T(2,128)} %all-to-all-done), kind=kLoop, calls=%fused_computation.86 | loop fusion | bytes 2097152 | tf_op jit(solution)/shard_map/slice | solution.py:68
  155.8 1.4 fusion.12
  157.2 1.7 slice.398
  158.9 1.7 slice.397
  160.6 1.7 slice.410
  162.3 1.7 slice.409
  164.0 1.9 %fusion.23 = (f32[32,2048]{1,0:T(8,128)}, f32[32,2048]{1,0:T(8,128)S(1)}) fusion(f32[32,2048]{1,0:T(8,128)} %slice.397, f32[32,2048]{1,0:T(8,128)} %slice.398, f32[32,2048]{1,0:T(8,128)} %slice.410, f32[32,2048]{1,0:T(8,128)} %slice.409), kind=kLoop, calls=%fused_computation.87 | loop fusion | flops 196608 | bytes 1572864 | tf_op jit(solution)/shard_map/vmap()/mul | solution.py:100
  166.9 1.6 slice.399
  171.5 2.3 %fusion.10 = bf16[1,128,2048]{2,1,0:T(8,128)(2,1)} fusion(f32[2048,128]{0,1:T(8,128)S(1)} %pad.112, f32[2048,128]{0,1:T(8,128)} %pad.113, f32[2048,128]{0,1:T(8,128)S(1)} %pad.98, f32[2048,128]{0,1:T(8,128)S(1)} %pad.99, f32[2048]{0:T(1024)S(1)} %bitcast.70), kind=kLoop, calls=%fused_computation.21 | loop fusion | flops 1310720 | bytes 4726784 | tf_op jit(solution)/shard_map/broadcast_in_dim | solution.py:140
  (146 shorter events, 16.3 us)
Async XLA Ops:
  6.5 17.2 %copy-start.4 = (bf16[1,128,2048]{2,1,0:T(8,128)(2,1)S(1)}, bf16[1,128,2048]{2,1,0:T(8,128)(2,1)}, u32[]{:S(2)}) copy-start(bf16[1,128,2048]{2,1,0:T(8,128)(2,1)} %param.5) | copy-start | bytes 1572868
  6.5 20.7 %copy-start.6 = (f32[2048]{0:T(1024)S(1)}, f32[2048]{0:T(1024)}, u32[]{:S(2)}) copy-start(f32[2048]{0:T(1024)} %param.8) | copy-start | bytes 24580
  6.5 20.7 %copy-start.5 = (bf16[4,2048]{1,0:T(4,128)(2,1)S(1)}, bf16[4,2048]{1,0:T(4,128)(2,1)}, u32[]{:S(2)}) copy-start(bf16[4,2048]{1,0:T(4,128)(2,1)} %param.6) | copy-start | bytes 49156
  6.5 36.9 %all-gather.5.cloned.1.call-start = ((), (), s32[]{:S(2)}) async-start(), calls=%async_computation.1 | async-start | bytes 1572864 | tf_op jit(solution)/shard_map/all_gather | solution.py:28
  21.5 54.8 %all-gather.7.cloned.1.call-start = ((), (), s32[]{:S(2)}) async-start(), calls=%async_computation.2 | async-start | bytes 1310720 | tf_op jit(solution)/shard_map/all_gather | solution.py:28
  23.7 8.6 %collective-permute-start = (bf16[2048,3]{0,1:T(4,128)(2,1)S(1)}, bf16[2048,3]{0,1:T(4,128)(2,1)S(1)}, u32[]{:S(2)}, u32[]{:S(2)}) collective-permute-start(bf16[2048,3]{0,1:T(4,128)(2,1)S(1)} %slice.422), channel_id=1, source_target_pairs={{0,8},{8,16},{16,24},{24,32},{32,40},{40,48},{48,56},{56,64},{64,7... | collective-permute-start | bytes 36872 | tf_op jit(solution)/shard_map/ppermute | solution.py:17
  91.6 3.0 %copy-start = (f32[2048,64]{0,1:T(8,128)S(1)}, f32[2048,64]{0,1:T(8,128)}, u32[]{:S(2)}) copy-start(f32[2048,64]{0,1:T(8,128)} %slice.334) | copy-start | bytes 1572868
  91.6 3.0 %copy-start.1 = (f32[2048,64]{0,1:T(8,128)S(1)}, f32[2048,64]{0,1:T(8,128)}, u32[]{:S(2)}) copy-start(f32[2048,64]{0,1:T(8,128)} %slice.333) | copy-start | bytes 1572868
  100.7 1.2 copy-start.2
  100.7 1.4 copy-start.3
  111.9 41.4 %all-to-all-start = ((f32[64,2,2048]{2,1,0:T(2,128)}), f32[64,2,2048]{2,1,0:T(2,128)}, u32[]{:S(2)}, u32[]{:S(2)}) async-start(f32[64,2,2048]{2,1,0:T(2,128)} %broadcast_in_dim.37), calls=%async_computation | async-start | bytes 2097152 | tf_op jit(solution)/shard_map/all_to_all | solution.py:55
Sparse Core Ops, SparseCore 0:
  21.6 21.7 all-gather.4
  45.5 30.7 all-gather.6
where the time goes:
time: 182 us; the launch traced here: 181 us
  waiting for transfers between devices  72.9 us (40%)
  local copies, waits for them, and re-layouts  42.2 us (23%)
  starting transfers between devices  17.1 us (9%)
  other arithmetic  16.5 us (9%)
  blocking collectives  16 us (9%)
  between operations  14.2 us (8%)
    all_gather x2, waiting for transfers between devices, gather_in_order(): pieces = lax.all_gather(pieces, axes[k], axis=0, tiled=True)  40.8 us
    all_to_all x1, waiting for transfers between devices, from_everyone(): return lax.all_to_all(copies, axis, split_axis=0, concat_axis=0, tiled=True)  27.8 us
    all_gather x2, blocking collectives, gather_in_order(): pieces = lax.all_gather(pieces, axes[k], axis=0, tiled=True)  16 us
    all_to_all x1, starting transfers between devices, from_everyone(): return lax.all_to_all(copies, axis, split_axis=0, concat_axis=0, tiled=True)  13.6 us
    slice x20, local copies, waits for them, and re-layouts, combined_pairwise(): part[side::2]  11.1 us
    slice x44, local copies, waits for them, and re-layouts, body(): decay_run, state = lax.associative_scan(combine, (decay, drive), axis=1)  10.8 us
    pad x24, local copies, waits for them, and re-layouts, body(): decay_run, state = lax.associative_scan(combine, (decay, drive), axis=1)  7.74 us
    ppermute x1, waiting for transfers between devices, passed_along(): return lax.ppermute(array, axis, pairs)  4.33 us
  transfers between devices with their start and end apart: 4, of which 4 were waited for; matrix products, arithmetic and copies ran while one was open for 2% of the time, Pallas kernels for 0%

commit v1 on v0

--- a/solution.py
+++ b/solution.py
@@ -25,7 +25,9 @@
 def gather_in_order(array, axes, sequence):
     pieces = array[None]
     for k in sequence:
-        pieces = lax.all_gather(pieces, axes[k], axis=0, tiled=True)
+        pieces = jnp.concatenate(
+            lax.all_to_all(jnp.stack([pieces] * lax.axis_size(axes[k])), axes[k], 0, 0), axis=0
+        )
     block = [lax.axis_size(axes[k]) for k in reversed(sequence)]
     pieces = pieces.reshape(*block, *array.shape)
     turned = sorted(range(len(sequence)), key=lambda place: sequence[len(sequence) - 1 - place])

time: 182 us -> 153 us (0.84)
  waiting for transfers between devices: 72.9 us -> 53.1 us
  starting transfers between devices: 17.1 us -> 31.5 us
  between operations: 14.2 us -> 0.84 us
  blocking collectives: 16 us -> 4.58 us
    all_gather x2 -> x0, waiting for transfers between devices: 40.8 us -> none  [gather_in_order(): pieces = lax.all_gather(pieces, axes[k], axis=0, tiled=True)]
    all_to_all x0 -> x3, waiting for transfers between devices: none -> 24.3 us  [gather_in_order(): lax.all_to_all(jnp.stack([pieces] * lax.axis_size(axes[k])), axes[k], 0, 0)]
    all_gather x2 -> x0, blocking collectives: 16 us -> none  [gather_in_order(): pieces = lax.all_gather(pieces, axes[k], axis=0, tiled=True)]
    all_to_all x0 -> x3, starting transfers between devices: none -> 12.1 us  [gather_in_order(): lax.all_to_all(jnp.stack([pieces] * lax.axis_size(axes[k])), axes[k], 0, 0)]
    all_to_all x0 -> x1, blocking collectives: none -> 4.58 us  [gather_in_order(): lax.all_to_all(jnp.stack([pieces] * lax.axis_size(axes[k])), axes[k], 0, 0)]
    ppermute x1, waiting for transfers between devices: 4.33 us -> 0.01 us  [passed_along(): return lax.ppermute(array, axis, pairs)]
    all_to_all x1, starting transfers between devices: 13.6 us -> 15.9 us  [from_everyone(): return lax.all_to_all(copies, axis, split_axis=0, concat_axis=0, tiled=True)]
    another operation x0 -> x3, local copies, waits for them, and re-layouts: none -> 2.2 us  [gather_in_order(): jnp.stack([pieces] * lax.axis_size(axes[k]))]
  transfers between devices with their start and end apart: 4 -> 5, of which waited for: 4 -> 4; matrix products, arithmetic and copies ran while one was open for 2% -> 4% of each run, Pallas kernels for 0% -> 0%
where the time goes in v1:
time: 153 us; the launch traced here: 151 us
  waiting for transfers between devices  53.1 us (35%)
  local copies, waits for them, and re-layouts  42.1 us (28%)
  starting transfers between devices  31.5 us (21%)
  other arithmetic  17.3 us (11%)
  blocking collectives  4.58 us (3%)
  matrix products  2.06 us (1%)
    all_to_all x1, waiting for transfers between devices, from_everyone(): return lax.all_to_all(copies, axis, split_axis=0, concat_axis=0, tiled=True)  28.8 us
    all_to_all x3, waiting for transfers between devices, gather_in_order(): lax.all_to_all(jnp.stack([pieces] * lax.axis_size(axes[k])), axes[k], 0, 0)  24.3 us
    all_to_all x1, starting transfers between devices, from_everyone(): return lax.all_to_all(copies, axis, split_axis=0, concat_axis=0, tiled=True)  15.9 us
    all_to_all x3, starting transfers between devices, gather_in_order(): lax.all_to_all(jnp.stack([pieces] * lax.axis_size(axes[k])), axes[k], 0, 0)  12.1 us
    slice x20, local copies, waits for them, and re-layouts, combined_pairwise(): part[side::2]  11.1 us
    slice x44, local copies, waits for them, and re-layouts, body(): decay_run, state = lax.associative_scan(combine, (decay, drive), axis=1)  10.8 us
    pad x24, local copies, waits for them, and re-layouts, body(): decay_run, state = lax.associative_scan(combine, (decay, drive), axis=1)  7.74 us
    all_to_all x1, blocking collectives, gather_in_order(): lax.all_to_all(jnp.stack([pieces] * lax.axis_size(axes[k])), axes[k], 0, 0)  4.58 us
  transfers between devices with their start and end apart: 5, of which 4 were waited for; matrix products, arithmetic and copies ran while one was open for 4% of the time, Pallas kernels for 0%

profile of v1, /device:TPU:8, one launch (start us, length us, event | category | flops | bytes accessed | tf_op | source)
XLA Modules:
  0.0 151.5 jit_solution(12761005664986415331)
XLA Ops:
  0.8 3.5 %collective-permute-start = (bf16[2048,3]{0,1:T(4,128)(2,1)S(1)}, bf16[2048,3]{0,1:T(4,128)(2,1)S(1)}, u32[]{:S(2)}, u32[]{:S(2)}) collective-permute-start(bf16[2048,3]{0,1:T(4,128)(2,1)S(1)} %slice.422), channel_id=1, source_target_pairs={{0,8},{8,16},{16,24},{24,32},{32,40},{40,48},{48,56},{56,64},{64,7... | collective-permute-start | bytes 36872 | tf_op jit(solution)/shard_map/ppermute | solution.py:17
  6.0 3.4 %all-to-all-start.2 = ((bf16[2,1,2,1,128,256]{5,4,2,3,1,0:T(8,128)(2,1)}), bf16[2,1,2,1,128,256]{5,4,2,3,1,0:T(8,128)(2,1)S(1)}, u32[]{:S(2)}, u32[]{:S(2)}) async-start(bf16[2,1,2,1,128,256]{5,4,2,3,1,0:T(8,128)(2,1)} %pad_maximum_fusion.3), calls=%async_computation.2 | async-start | bytes 524288 | tf_op jit(solution)/shard_map/all_to_all | solution.py:29
  9.6 1.4 all-to-all-done.2
  11.9 4.3 %all-to-all-start = ((bf16[4,1,2,1,128,256]{4,5,2,3,1,0:T(8,128)(2,1)}), bf16[4,1,2,1,128,256]{4,5,2,3,1,0:T(8,128)(2,1)S(1)}, u32[]{:S(2)}, u32[]{:S(2)}) async-start(bf16[4,1,2,1,128,256]{4,5,2,3,1,0:T(8,128)(2,1)} %stack.12), calls=%async_computation | async-start | bytes 1048576 | tf_op jit(solution)/shard_map/all_to_all | solution.py:29
  16.4 9.6 %all-to-all-done = bf16[4,1,2,1,128,256]{4,5,2,3,1,0:T(8,128)(2,1)S(1)} async-done(((bf16[4,1,2,1,128,256]{4,5,2,3,1,0:T(8,128)(2,1)}), bf16[4,1,2,1,128,256]{4,5,2,3,1,0:T(8,128)(2,1)S(1)}, u32[]{:S(2)}, u32[]{:S(2)}) %all-to-all-start) | async-done | bytes 524320 | tf_op jit(solution)/shard_map/all_to_all | solution.py:29
  26.0 4.6 %all_to_all.25 = bf16[2,4,2,1,128,256]{4,5,2,1,3,0:T(8,128)(2,1)S(1)} all-to-all(bf16[2,4,2,1,128,256]{4,5,2,1,3,0:T(8,128)(2,1)S(1)} %pad_maximum_fusion), channel_id=1, replica_groups=mesh['sp'=64,'dp_0'=4,'dp_1'=2] {'dp_1'}, dimensions={0} | all-to-all | bytes 2097152 | tf_op jit(solution)/shard_map/all_to_all | solution.py:29
  31.8 4.4 %all-to-all-start.3 = ((bf16[4,2,2,1,128,256]{4,5,2,1,3,0:T(8,128)(2,1)}), bf16[4,2,2,1,128,256]{4,5,2,1,3,0:T(8,128)(2,1)}, u32[]{:S(2)}, u32[]{:S(2)}) async-start(bf16[4,2,2,1,128,256]{4,5,2,1,3,0:T(8,128)(2,1)} %stack.15), calls=%async_computation.3 | async-start | bytes 2097152 | tf_op jit(solution)/shard_map/all_to_all | solution.py:29
  38.6 13.3 %all-to-all-done.3 = bf16[4,2,2,1,128,256]{4,5,2,1,3,0:T(8,128)(2,1)} async-done(((bf16[4,2,2,1,128,256]{4,5,2,1,3,0:T(8,128)(2,1)}), bf16[4,2,2,1,128,256]{4,5,2,1,3,0:T(8,128)(2,1)}, u32[]{:S(2)}, u32[]{:S(2)}) %all-to-all-start.3) | async-done | bytes 1048608 | tf_op jit(solution)/shard_map/all_to_all | solution.py:29
  51.9 2.1 %fusion.4 = bf16[2,8,256,128]{3,2,0,1:T(8,128)(2,1)S(1)} fusion(bf16[8,256,128,1]{2,1,3,0:T(8,128)(2,1)} %bitcast.60, bf16[8,2,1,128,256]{3,4,1,0,2:T(8,128)(2,1)} %bitcast.7, bf16[8,2,1,128,256]{3,4,1,0,2:T(8,128)(2,1)S(1)} %bitcast.56), kind=kOutput, calls=%fused_computation.5 | convolution fusion | flops 273154048 | bytes 3670016 | tf_op jit(solution)/shard_map/hit,ghij->ghjt/dot_general | solution.py:127
  54.5 1.3 copy.16
  57.2 2.8 %convert_multiply_fusion = (f32[2048,128]{0,1:T(8,128)S(1)}, f32[2048,128]{0,1:T(8,128)S(1)}) fusion(f32[2048,128]{0,1:T(8,128)} %copy.16, f32[2048,128]{0,1:T(8,128)} %copy.15, f32[2048]{0:T(1024)S(1)} %compare_select_fusion, f32[128]{0:T(128)S(1)} %multiply_bitcast_fusion, f32[2048,131]{0,1:T(8,128)S(1)} %maximum_convert_fusion, f32[2048]{0:T(1024)S(1)} %bitcast.68, ...), kind=kLoop, calls=%fused_computation.16 | loop fusion | flops 3932160 | bytes 8430080 | tf_op jit(solution)/shard_map/mul | solution.py:110
  60.0 1.5 %slice.380 = f32[2048,63]{0,1:T(8,128)} slice(f32[2048,128]{0,1:T(8,128)S(1)} %get-tuple-element.5), slice={[0:2048:1], [2:128:2]} | slice | bytes 1032192 | tf_op jit(solution)/shard_map/slice | solution.py:138
  61.5 1.5 slice.334
  63.0 1.5 slice.333
  64.4 1.5 slice.336
  65.9 1.5 slice.332
  67.4 1.5 %slice.331 = f32[2048,63]{0,1:T(8,128)} slice(f32[2048,128]{0,1:T(8,128)S(1)} %get-tuple-element.6), slice={[0:2048:1], [2:128:2]} | slice | bytes 1032192 | tf_op jit(solution)/shard_map/slice | solution.py:138
  68.9 1.3 multiply_add_fusion
  77.0 2.1 %pad.99 = f32[2048,128]{0,1:T(8,128)S(1)} pad(f32[2048,64]{0,1:T(8,128)} %add.213, f32[]{:T(128)} %constant.8.clone.1), padding=0_0_0x1_0_1 | pad | bytes 1572868 | tf_op jit(solution)/shard_map/pad | solution.py:138
  79.1 4.6 %pad.113 = f32[2048,128]{0,1:T(8,128)} pad(f32[2048,64]{0,1:T(8,128)} %add.221, f32[]{:T(128)} %constant.8.clone.1), padding=0_0_0x1_0_1 | pad | bytes 1572868 | tf_op jit(solution)/shard_map/pad | solution.py:138
  84.7 1.5 broadcast_in_dim.29
  86.2 15.9 %all-to-all-start.4 = ((f32[64,2,2048]{2,1,0:T(2,128)}), f32[64,2,2048]{2,1,0:T(2,128)}, u32[]{:S(2)}, u32[]{:S(2)}) async-start(f32[64,2,2048]{2,1,0:T(2,128)} %broadcast_in_dim.29), calls=%async_computation.4 | async-start | bytes 2097152 | tf_op jit(solution)/shard_map/all_to_all | solution.py:57
  102.1 28.8 %all-to-all-done.4 = f32[64,2,2048]{2,1,0:T(2,128)} async-done(((f32[64,2,2048]{2,1,0:T(2,128)}), f32[64,2,2048]{2,1,0:T(2,128)}, u32[]{:S(2)}, u32[]{:S(2)}) %all-to-all-start.4) | async-done | bytes 1048608 | tf_op jit(solution)/shard_map/all_to_all | solution.py:57
  130.9 2.6 %fusion.22 = (f32[64,1,2048]{2,1,0:T(1,128)S(1)}, f32[64,1,2048]{2,1,0:T(1,128)S(1)}) fusion(f32[64,2,2048]{2,1,0:T(2,128)} %all-to-all-done.4), kind=kLoop, calls=%fused_computation.90 | loop fusion | bytes 2097152 | tf_op jit(solution)/shard_map/slice | solution.py:70
  133.5 1.4 fusion.12
  134.9 1.7 %slice.398 = f32[32,2048]{1,0:T(8,128)} slice(f32[64,2048]{1,0:T(8,128)} %get-tuple-element.55), slice={[1:64:2], [0:2048:1]} | slice | bytes 524288 | tf_op jit(solution)/shard_map/slice | solution.py:80
  136.6 1.7 %slice.397 = f32[32,2048]{1,0:T(8,128)} slice(f32[64,2048]{1,0:T(8,128)} %get-tuple-element.55), slice={[0:64:2], [0:2048:1]} | slice | bytes 524288 | tf_op jit(solution)/shard_map/slice | solution.py:80
  138.3 1.7 %slice.410 = f32[32,2048]{1,0:T(8,128)} slice(f32[64,2048]{1,0:T(8,128)} %get-tuple-element.56), slice={[1:64:2], [0:2048:1]} | slice | bytes 524288 | tf_op jit(solution)/shard_map/slice | solution.py:80
  140.0 1.7 %slice.409 = f32[32,2048]{1,0:T(8,128)} slice(f32[64,2048]{1,0:T(8,128)} %get-tuple-element.56), slice={[0:64:2], [0:2048:1]} | slice | bytes 524288 | tf_op jit(solution)/shard_map/slice | solution.py:80
  141.7 1.9 %fusion.23 = (f32[32,2048]{1,0:T(8,128)}, f32[32,2048]{1,0:T(8,128)S(1)}) fusion(f32[32,2048]{1,0:T(8,128)} %slice.397, f32[32,2048]{1,0:T(8,128)} %slice.398, f32[32,2048]{1,0:T(8,128)} %slice.410, f32[32,2048]{1,0:T(8,128)} %slice.409), kind=kLoop, calls=%fused_computation.91 | loop fusion | flops 196608 | bytes 1572864 | tf_op jit(solution)/shard_map/vmap()/mul | solution.py:102
  144.6 1.6 %slice.399 = f32[16,2048]{1,0:T(8,128)} slice(f32[32,2048]{1,0:T(8,128)} %get-tuple-element.15), slice={[0:32:2], [0:2048:1]} | slice | bytes 262144 | tf_op jit(solution)/shard_map/slice | solution.py:80
  149.1 2.3 %fusion.10 = bf16[1,128,2048]{2,1,0:T(8,128)(2,1)} fusion(f32[2048,128]{0,1:T(8,128)S(1)} %pad.112, f32[2048,128]{0,1:T(8,128)} %pad.113, f32[2048,128]{0,1:T(8,128)S(1)} %pad.98, f32[2048,128]{0,1:T(8,128)S(1)} %pad.99, f32[2048]{0:T(1024)S(1)} %bitcast.69), kind=kLoop, calls=%fused_computation.22 | loop fusion | flops 1310720 | bytes 4726784 | tf_op jit(solution)/shard_map/broadcast_in_dim | solution.py:142
  (150 shorter events, 20.1 us)
Async XLA Ops:
  0.0 9.5 %copy-start.6 = (f32[2048]{0:T(1024)S(1)}, f32[2048]{0:T(1024)}, u32[]{:S(2)}) copy-start(f32[2048]{0:T(1024)} %param.8) | copy-start | bytes 24580
  0.8 36.0 %collective-permute-start = (bf16[2048,3]{0,1:T(4,128)(2,1)S(1)}, bf16[2048,3]{0,1:T(4,128)(2,1)S(1)}, u32[]{:S(2)}, u32[]{:S(2)}) collective-permute-start(bf16[2048,3]{0,1:T(4,128)(2,1)S(1)} %slice.422), channel_id=1, source_target_pairs={{0,8},{8,16},{16,24},{24,32},{32,40},{40,48},{48,56},{56,64},{64,7... | collective-permute-start | bytes 36872 | tf_op jit(solution)/shard_map/ppermute | solution.py:17
  6.0 5.0 %all-to-all-start.2 = ((bf16[2,1,2,1,128,256]{5,4,2,3,1,0:T(8,128)(2,1)}), bf16[2,1,2,1,128,256]{5,4,2,3,1,0:T(8,128)(2,1)S(1)}, u32[]{:S(2)}, u32[]{:S(2)}) async-start(bf16[2,1,2,1,128,256]{5,4,2,3,1,0:T(8,128)(2,1)} %pad_maximum_fusion.3), calls=%async_computation.2 | async-start | bytes 524288 | tf_op jit(solution)/shard_map/all_to_all | solution.py:29
  9.6 6.7 %copy-start.5 = (bf16[4,2048]{1,0:T(4,128)(2,1)S(1)}, bf16[4,2048]{1,0:T(4,128)(2,1)}, u32[]{:S(2)}) copy-start(bf16[4,2048]{1,0:T(4,128)(2,1)} %param.6) | copy-start | bytes 49156
  11.9 14.1 %all-to-all-start = ((bf16[4,1,2,1,128,256]{4,5,2,3,1,0:T(8,128)(2,1)}), bf16[4,1,2,1,128,256]{4,5,2,3,1,0:T(8,128)(2,1)S(1)}, u32[]{:S(2)}, u32[]{:S(2)}) async-start(bf16[4,1,2,1,128,256]{4,5,2,3,1,0:T(8,128)(2,1)} %stack.12), calls=%async_computation | async-start | bytes 1048576 | tf_op jit(solution)/shard_map/all_to_all | solution.py:29
  31.8 5.1 %copy-start.4 = (bf16[1,128,2048]{2,1,0:T(8,128)(2,1)S(1)}, bf16[1,128,2048]{2,1,0:T(8,128)(2,1)}, u32[]{:S(2)}) copy-start(bf16[1,128,2048]{2,1,0:T(8,128)(2,1)} %param.5) | copy-start | bytes 1572868
  31.8 20.1 %all-to-all-start.3 = ((bf16[4,2,2,1,128,256]{4,5,2,1,3,0:T(8,128)(2,1)}), bf16[4,2,2,1,128,256]{4,5,2,1,3,0:T(8,128)(2,1)}, u32[]{:S(2)}, u32[]{:S(2)}) async-start(bf16[4,2,2,1,128,256]{4,5,2,1,3,0:T(8,128)(2,1)} %stack.15), calls=%async_computation.3 | async-start | bytes 2097152 | tf_op jit(solution)/shard_map/all_to_all | solution.py:29
  65.9 3.0 %copy-start = (f32[2048,64]{0,1:T(8,128)S(1)}, f32[2048,64]{0,1:T(8,128)}, u32[]{:S(2)}) copy-start(f32[2048,64]{0,1:T(8,128)} %slice.334) | copy-start | bytes 1572868
  65.9 3.0 %copy-start.1 = (f32[2048,64]{0,1:T(8,128)S(1)}, f32[2048,64]{0,1:T(8,128)}, u32[]{:S(2)}) copy-start(f32[2048,64]{0,1:T(8,128)} %slice.333) | copy-start | bytes 1572868
  75.0 1.2 copy-start.2
  75.0 1.4 copy-start.3
  86.2 44.7 %all-to-all-start.4 = ((f32[64,2,2048]{2,1,0:T(2,128)}), f32[64,2,2048]{2,1,0:T(2,128)}, u32[]{:S(2)}, u32[]{:S(2)}) async-start(f32[64,2,2048]{2,1,0:T(2,128)} %broadcast_in_dim.29), calls=%async_computation.4 | async-start | bytes 2097152 | tf_op jit(solution)/shard_map/all_to_all | solution.py:57
